TPU v7x, 256 devices: a whole 4x4x8 slice. The times are simulated.
256 devices in a mesh: sp: 64 (over z, x, core), tp: 4 (over y).
Axes of the slice: x: 4, y: 4, z: 8, core: 2. Of those that a mesh axis runs over, the one named last changes fastest.
Arguments:
- tokens: bfloat16 [65536, 2048], P('sp'), may hold values from -8 to 8
- norm_gain: float32 [2048], replicated, may hold values from 0.1 to 1.9
- query_weight: bfloat16 [2048, 512], P(None, 'tp'), may hold values from -40 to 40
- key_weight: bfloat16 [2048, 256], P(None, 'tp'), may hold values from -1 to 1
- value_weight: bfloat16 [2048, 256], P(None, 'tp'), may hold values from -0.125 to 0.125
- sink_logits: float32 [8], P('tp'), may hold values from 1 to 6
- conv_in_weight: bfloat16 [2048, 512], P(None, 'tp'), may hold values from -0.125 to 0.125
- conv_gate_weight: bfloat16 [2048, 512], P(None, 'tp'), may hold values from -0.125 to 0.125
- conv_taps: bfloat16 [31, 512], replicated, may hold values from -1 to 1
- conv_gain: float32 [512], replicated, may hold values from 0.1 to 1.9
- point_weight: bfloat16 [512, 512], replicated, may hold values from -0.25 to 0.25
- output_gain: float32 [1024], replicated, may hold values from 0.1 to 1.9
- output_weight: bfloat16 [1024, 2048], P('sp'), may hold values from -0.1875 to 0.1875
Outputs:
- mixed_output: bfloat16 [65536, 2048], P(('sp', 'tp'))
All inputs are finite; a program needn't handle non-finite values.
Results may differ from a plain program's by a relative error of at most 0.0087.
Values may be sent and summed in bfloat16 or wider, within the bound.
A program may use at most 64 MiB of HBM per device.

v0:
```python
import jax
import jax.numpy as jnp
from jax import lax
from jax.sharding import Mesh
from jax.sharding import PartitionSpec as P

HEADS = 8
KV_HEADS = 4
HEAD_DIM = 64
WINDOW = 128
CONV_WIDTH = 31
SP = ("sp_0", "sp_1", "sp_2")
SP_TP = ("sp_0", "sp_1", "sp_2", "tp")


NORM_EPSILON = 1e-06
MASKED_SCORE = -1e30


def from_behind(block, axis, distance):
    devices = range(lax.axis_size(axis))
    route = [(i - distance, i) for i in devices if i - distance in devices]
    return lax.ppermute(block, axis, route)


def laid_out(tiles, dim):
    dims = list(tiles.shape[1:])
    dims[dim] *= tiles.shape[0]
    return jnp.moveaxis(tiles, 0, dim).reshape(dims)


def stacked_from(value, axes, turns):
    tiles = value[None]
    for k in turns:
        tiles = lax.all_gather(tiles, axes[k], axis=0, tiled=True)
    carried = [lax.axis_size(axes[k]) for k in reversed(turns)]
    tiles = tiles.reshape(*carried, *value.shape)
    turned = sorted(range(len(turns)), key=lambda place: turns[len(turns) - 1 - place])
    return tiles.transpose(*turned, *range(len(turns), tiles.ndim)).reshape(-1, *value.shape)


def gathered_by_axis(value, axes, turns, dim):
    return laid_out(stacked_from(value, axes, turns), dim)


def rms_rows(values, scale_gain):
    return (
        values
        * lax.rsqrt(jnp.mean(values * values, axis=-1, keepdims=True) + NORM_EPSILON)
        * scale_gain
    )


def depthwise(current, earlier_rows, tap_weights):
    extended = jnp.concatenate([earlier_rows, current], axis=0).astype(jnp.float32)
    tap_floats = tap_weights.astype(jnp.float32)
    row_count = current.shape[0]
    result = jnp.zeros(current.shape, jnp.float32)
    for tap_index in range(CONV_WIDTH):
        result = result + tap_floats[tap_index] * extended[tap_index : tap_index + row_count]
    return lax.optimization_barrier(result.astype(jnp.bfloat16))


def layer_activate(conv_rows, channel_gain):
    widened = conv_rows.astype(jnp.float32)
    centered = widened - jnp.mean(widened, axis=-1, keepdims=True)
    scaled = (
        centered
        * lax.rsqrt(jnp.mean(centered * centered, axis=-1, keepdims=True) + NORM_EPSILON)
        * channel_gain
    )
    return jax.nn.silu(scaled).astype(jnp.bfloat16)


def merge_groups(attended, pointwise, output_gain):
    head_width = attended.shape[1]
    return jnp.concatenate(
        [
            rms_rows(attended.astype(jnp.float32), output_gain[:head_width]),
            rms_rows(pointwise, output_gain[head_width:]),
        ],
        axis=1,
    ).astype(jnp.bfloat16)


def window_attention(queries, key_values, earlier_pairs, sinks_here, offset):
    row_count = queries.shape[0]
    block_count = row_count // WINDOW
    group_size = HEADS // KV_HEADS
    key_heads = key_values.shape[1] // (2 * HEAD_DIM)
    extended = jnp.concatenate([earlier_pairs, key_values], axis=0)
    extended = extended.reshape(block_count + 1, WINDOW, 2, key_heads, HEAD_DIM)
    key_value_band = jnp.concatenate([extended[:-1], extended[1:]], axis=1)
    key_band = key_value_band[:, :, 0]
    value_band = key_value_band[:, :, 1]
    grouped = queries.reshape(block_count, WINDOW, key_heads, group_size, HEAD_DIM)
    scores = jnp.einsum(
        "nqkgd,njkd->nkgqj", grouped, key_band, preferred_element_type=jnp.float32
    ) * HEAD_DIM ** (-0.5)
    query_index = lax.broadcasted_iota(jnp.int32, (WINDOW, 2 * WINDOW), 0)
    key_index = lax.broadcasted_iota(jnp.int32, (WINDOW, 2 * WINDOW), 1)
    distance = WINDOW + query_index - key_index
    in_window = (distance >= 0) & (distance < WINDOW)
    block_start = offset + jnp.arange(block_count, dtype=jnp.int32) * WINDOW - WINDOW
    allowed = in_window[None] & (block_start[:, None, None] + key_index[None] >= 0)
    scores = jnp.where(allowed[:, None, None], scores, MASKED_SCORE)
    sink_logit = sinks_here.reshape(key_heads, group_size)[None, :, :, None, None]
    row_peak = jnp.maximum(jnp.max(scores, axis=-1, keepdims=True), sink_logit)
    raised = jnp.exp(scores - row_peak)
    denominator = jnp.sum(raised, axis=-1, keepdims=True) + jnp.exp(sink_logit - row_peak)
    weights = (raised / denominator).astype(jnp.bfloat16)
    attended = jnp.einsum(
        "nkgqj,njkd->nqkgd", weights, value_band, preferred_element_type=jnp.float32
    )
    return attended.astype(jnp.bfloat16).reshape(row_count, key_heads * group_size * HEAD_DIM)


def on_device(
    tokens,
    norm_gain,
    query_weight,
    key_weight,
    value_weight,
    sink_logits,
    conv_in_weight,
    conv_gate_weight,
    conv_taps,
    conv_gain,
    point_weight,
    output_gain,
    output_weight,
):
    local_rows = tokens.shape[0]
    narrow_index = lax.axis_index("tp")
    offset = lax.axis_index(SP) * local_rows
    normed = rms_rows(tokens.astype(jnp.float32), norm_gain).astype(jnp.bfloat16)
    queries = jnp.dot(normed, query_weight, preferred_element_type=jnp.float32).astype(jnp.bfloat16)
    key_part = jnp.dot(normed, key_weight, preferred_element_type=jnp.float32).astype(jnp.bfloat16)
    value_part = jnp.dot(normed, value_weight, preferred_element_type=jnp.float32).astype(
        jnp.bfloat16
    )
    key_values = jnp.concatenate([key_part, value_part], axis=1)
    conv_in = jnp.dot(normed, conv_in_weight, preferred_element_type=jnp.float32)
    conv_gate = jnp.dot(normed, conv_gate_weight, preferred_element_type=jnp.float32)
    gated_rows = (conv_in * jax.nn.sigmoid(conv_gate)).astype(jnp.bfloat16)
    earlier_pairs = from_behind(key_values[local_rows - WINDOW :], SP, 1)
    conv_share = gated_rows.shape[1]
    local_taps = lax.dynamic_slice_in_dim(conv_taps, narrow_index * conv_share, conv_share, 1)
    earlier_gated = from_behind(gated_rows[local_rows - (CONV_WIDTH - 1) :], SP, 1)
    second = depthwise(gated_rows, earlier_gated, local_taps)
    attended = window_attention(queries, key_values, earlier_pairs, sink_logits, offset)
    head_rows, second_rows = (
        lax.all_to_all(attended, "tp", split_axis=0, concat_axis=1, tiled=True),
        lax.all_to_all(second, "tp", split_axis=0, concat_axis=1, tiled=True),
    )
    activated = layer_activate(second_rows, conv_gain)
    pointwise = jnp.dot(activated, point_weight, preferred_element_type=jnp.float32)
    merged = merge_groups(head_rows, pointwise, output_gain)
    projected = jnp.dot(
        merged,
        gathered_by_axis(output_weight, SP, (1, 0, 2), 0),
        preferred_element_type=jnp.float32,
    )
    return projected.astype(jnp.bfloat16)


def solution(mesh):
    split = Mesh(mesh.devices.reshape(8, 4, 2, mesh.shape["tp"]), ("sp_0", "sp_1", "sp_2", "tp"))
    in_specs = (
        P(SP, None),
        P(),
        P(None, "tp"),
        P(None, "tp"),
        P(None, "tp"),
        P("tp"),
        P(None, "tp"),
        P(None, "tp"),
        P(),
        P(),
        P(),
        P(),
        P(SP, None),
    )
    out_specs = P(SP_TP, None)
    return jax.shard_map(
        on_device, mesh=split, in_specs=in_specs, out_specs=out_specs, check_vma=False
    )
```

profile of v0, /device:TPU:1, one launch (start us, length us, event | category | flops | bytes accessed | tf_op | source)
XLA Modules:
  0.0 96.1 jit_solution(10272856138030414230)
XLA Ops:
  6.5 0.0 copy-start
  6.5 0.0 all-gather.4.cloned.1.call-start
  6.5 12.5 %all-gather = bf16[64,2048]{1,0:T(8,128)(2,1)} all-gather(bf16[16,2048]{1,0:T(8,128)(2,1)} %param.25), channel_id=2, replica_groups=mesh['sp_0'=8,'sp_1'=4,'sp_2'=2,'tp'=4] {'sp_1'}, dimensions={0}, use_global_device_ids=true | all-gather | bytes 327680 | tf_op jit(solution)/shard_map/all_gather | solution.py:35
  19.1 0.0 all-gather.4.cloned.1.call-update
  19.1 0.0 copy-start.2
  19.1 3.2 %fusion = f32[1024]{0:T(1024)S(1)} fusion(bf16[1024,2048]{1,0:T(8,128)(2,1)} %param.13), kind=kLoop, calls=%fused_computation.2 | loop fusion | flops 6290432 | bytes 4198400 | tf_op jit(solution)/shard_map/reduce_sum | solution.py:49
  22.3 0.0 copy-done.6
  22.3 0.2 copy-done.2
  22.5 1.0 %fusion.2 = bf16[1024,2048]{1,0:T(8,128)(2,1)S(1)} fusion(bf16[1024,2048]{1,0:T(8,128)(2,1)S(1)} %copy-done.2, f32[2048]{0:T(1024)S(1)} %copy-done.6, f32[1024]{0:T(1024)S(1)} %add_rsqrt_fusion), kind=kLoop, calls=%fused_computation.4 | loop fusion | flops 8388608 | bytes 8400896 | tf_op jit(solution)/shard_map/convert_element_type | solution.py:136
  23.6 0.0 copy-done.4
  23.6 0.0 copy-start.1
  23.6 0.0 copy-start.5
  23.6 1.4 %convolution_convert_fusion.3 = bf16[1024,64]{0,1:T(8,128)(2,1)S(1)} fusion(bf16[1024,2048]{1,0:T(8,128)(2,1)S(1)} %fusion.2, bf16[2048,64]{0,1:T(8,128)(2,1)S(1)} %copy-done.4), kind=kOutput, calls=%fused_computation.19 | convolution fusion | flops 268500992 | bytes 4587520 | tf_op jit(solution)/shard_map/dot_general | solution.py:139
  25.0 0.0 copy-done.5
  25.0 0.0 copy-start.10
  25.0 1.4 %convolution_convert_fusion.4 = bf16[1024,64]{0,1:T(8,128)(2,1)S(1)} fusion(bf16[1024,2048]{1,0:T(8,128)(2,1)S(1)} %fusion.2, bf16[2048,64]{0,1:T(8,128)(2,1)S(1)} %copy-done.5), kind=kOutput, calls=%fused_computation.20 | convolution fusion | flops 268500992 | bytes 4587520 | tf_op jit(solution)/shard_map/dot_general | solution.py:138
  26.4 0.0 copy-start.3
  26.4 5.9 %collective-permute-start = (bf16[128,128]{0,1:T(8,128)(2,1)S(1)}, bf16[128,128]{0,1:T(8,128)(2,1)S(1)}, u32[]{:S(2)}, u32[]{:S(2)}) collective-permute-start(bf16[128,128]{0,1:T(8,128)(2,1)S(1)} %fusion.53), channel_id=1, source_target_pairs={{0,4},{4,8},{8,12},{12,16},{16,20},{20,24},{24,28},{28,32},{32,36}... | collective-permute-start | bytes 98312 | tf_op jit(solution)/shard_map/ppermute | solution.py:23
  32.4 1.3 %fusion.6 = f32[1024,128]{1,0:T(8,128)S(1)} fusion(bf16[1024,2048]{1,0:T(8,128)(2,1)S(1)} %fusion.2, bf16[2048,128]{1,0:T(8,128)(2,1)S(1)} %copy-done.10), kind=kOutput, calls=%fused_computation.14 | convolution fusion | flops 537264128 | bytes 5242880 | tf_op jit(solution)/shard_map/dot_general | solution.py:144
  33.7 0.0 copy-start.11
  33.7 1.3 %fusion.7 = bf16[1024,128]{1,0:T(8,128)(2,1)S(1)} fusion(f32[1024,128]{1,0:T(8,128)S(1)} %fusion.6, bf16[1024,2048]{1,0:T(8,128)(2,1)S(1)} %fusion.2, bf16[2048,128]{1,0:T(8,128)(2,1)S(1)} %copy-done.3), kind=kOutput, calls=%fused_computation.16 | convolution fusion | flops 537133056 | bytes 5505024 | tf_op jit(solution)/shard_map/dot_general | solution.py:143
  34.9 0.0 copy-start.7
  35.0 1.9 %collective-permute-start.1 = (bf16[30,128]{1,0:T(8,128)(2,1)S(1)}, bf16[30,128]{1,0:T(8,128)(2,1)S(1)}, u32[]{:S(2)}, u32[]{:S(2)}) collective-permute-start(bf16[30,128]{1,0:T(8,128)(2,1)S(1)} %slice.290), channel_id=1, source_target_pairs={{0,4},{4,8},{8,12},{12,16},{16,20},{20,24},{24,28},{28,32},{32,36}... | collective-permute-start | bytes 23048 | tf_op jit(solution)/shard_map/ppermute | solution.py:23
  36.9 0.7 dynamic-slice_convert_fusion
  37.7 0.3 fusion.10
  38.0 0.0 copy-done.11
  38.0 3.4 %convolution_convert_fusion.2 = bf16[1024,128]{1,0:T(8,128)(2,1)S(1)} fusion(bf16[1024,2048]{1,0:T(8,128)(2,1)} %copy-done.1, bf16[2048,128]{1,0:T(8,128)(2,1)S(1)} %copy-done.11), kind=kOutput, calls=%fused_computation.17 | convolution fusion | flops 537001984 | bytes 4980736 | tf_op jit(solution)/shard_map/dot_general | solution.py:137
  41.5 0.2 reshape.151
  41.7 0.0 collective-permute-done.1
  41.7 0.1 maximum_convert_fusion
  41.8 2.1 %fusion.12 = bf16[1024,128]{1,0:T(8,128)(2,1)S(1)} fusion(f32[1054,128]{1,0:T(8,128)S(1)} %maximum_convert_fusion, f32[128]{0:T(128)S(1)} %get-tuple-element.8, f32[128]{0:T(128)S(1)} %get-tuple-element.9, f32[128]{0:T(128)S(1)} %get-tuple-element.10, f32[128]{0:T(128)S(1)} %get-tuple-element.11, f32[128]{0:T(128)S(1)} %get-tuple-element.12, ...), kind=kLoop, calls=%fused_computation.26 | loop fusion | flops 8126464 | bytes 16530944 | tf_op jit(solution)/shard_map/convert_element_type | solution.py:61
  43.9 0.9 copy.43
  44.8 3.7 %all-to-all-start.1 = ((bf16[4,256,128]{1,2,0:T(8,128)(2,1)}), bf16[4,256,128]{1,2,0:T(8,128)(2,1)S(1)}, u32[]{:S(2)}, u32[]{:S(2)}) async-start(bf16[4,256,128]{1,2,0:T(8,128)(2,1)} %copy.43), calls=%async_computation.1 | async-start | bytes 524288 | tf_op jit(solution)/shard_map/all_to_all | solution.py:154
  48.5 11.7 %all-gather.4.cloned.1.call-done = bf16[32,16,2048]{2,1,0:T(8,128)(2,1)} async-done(((bf16[4,16,2048]{2,1,0:T(8,128)(2,1)}), bf16[32,16,2048]{2,1,0:T(8,128)(2,1)}) %all-gather.4.cloned.1.call-update) | async-done | bytes 2097168 | tf_op jit(solution)/shard_map/all_gather | solution.py:35
  60.2 0.0 all-gather.6.cloned.1.call-update
  60.3 0.0 collective-permute-done
  60.3 0.1 fusion.48
  60.5 0.1 copy_dynamic-update-slice_fusion
  60.6 0.6 fusion.56
  61.2 0.0 copy-done.9
  61.2 0.1 broadcast_maximum_fusion
  61.3 0.3 fusion.3
  61.6 0.1 exponential_add_fusion
  61.7 0.0 copy-start.8
  61.7 0.5 fusion.8
  62.2 0.2 copy.40
  62.4 0.2 all_to_all.20
  62.5 0.7 copy.41
  63.3 0.0 all-to-all-done.1
  63.3 4.0 %all-to-all-start = ((bf16[4,256,128]{1,2,0:T(8,128)(2,1)}), bf16[4,256,128]{1,2,0:T(8,128)(2,1)S(1)}, u32[]{:S(2)}, u32[]{:S(2)}) async-start(bf16[4,256,128]{1,2,0:T(8,128)(2,1)} %copy.41), calls=%async_computation | async-start | bytes 524288 | tf_op jit(solution)/shard_map/all_to_all | solution.py:153
  67.2 0.1 convert_reduce_fusion
  67.3 0.1 multiply_reduce_fusion.1
  67.5 0.0 copy-done.8
  67.5 0.2 multiply_convert_fusion.1
  67.7 0.0 copy-done
  67.7 0.4 multiply_reduce_fusion
  68.1 0.1 multiply_convert_fusion
  68.2 4.5 %all-to-all-done = bf16[4,256,128]{1,2,0:T(8,128)(2,1)S(1)} async-done(((bf16[4,256,128]{1,2,0:T(8,128)(2,1)}), bf16[4,256,128]{1,2,0:T(8,128)(2,1)S(1)}, u32[]{:S(2)}, u32[]{:S(2)}) %all-to-all-start) | async-done | bytes 262176 | tf_op jit(solution)/shard_map/all_to_all | solution.py:153
  72.8 0.2 copy.50
  73.0 0.1 multiply_reduce_fusion.2
  73.1 0.1 multiply_convert_fusion.2
  73.2 11.3 %all-gather.6.cloned.1.call-done = bf16[64,16,2048]{2,1,0:T(8,128)(2,1)} async-done(((bf16[32,16,2048]{2,1,0:T(8,128)(2,1)}), bf16[64,16,2048]{2,1,0:T(8,128)(2,1)}) %all-gather.6.cloned.1.call-update) | async-done | bytes 4194320 | tf_op jit(solution)/shard_map/all_gather | solution.py:35
  84.6 2.5 %copy.44 = bf16[8,4,2,16,2048]{4,3,2,1,0:T(8,128)(2,1)S(1)} copy(bf16[8,4,2,16,2048]{4,3,1,0,2:T(8,128)(2,1)} %bitcast.137) | data formatting | bytes 8388608 | tf_op jit(solution)/shard_map/transpose | solution.py:39
  87.1 2.2 %convolution_convert_fusion = bf16[256,2048]{1,0:T(8,128)(2,1)} fusion(bf16[1024,2048]{1,0:T(8,128)(2,1)S(1)} %bitcast.138, bf16[256,512]{1,0:T(8,128)(2,1)S(1)} %multiply_convert_fusion, bf16[256,512]{1,0:T(8,128)(2,1)S(1)} %multiply_convert_fusion.2), kind=kOutput, calls=%fused_computation.5 | convolution fusion | flops 1075314688 | bytes 5767168 | tf_op jit(solution)/shard_map/dot_general | solution.py:159
  (25 shorter events, 0.3 us)
Async XLA Ops:
  6.5 61.2 %copy-start = (bf16[512,512]{1,0:T(8,128)(2,1)S(1)}, bf16[512,512]{1,0:T(8,128)(2,1)}, u32[]{:S(2)}) copy-start(bf16[512,512]{1,0:T(8,128)(2,1)} %param.23) | copy-start | bytes 1572868
  6.5 15.8 %copy-start.6 = (f32[2048]{0:T(1024)S(1)}, f32[2048]{0:T(1024)}, u32[]{:S(2)}) copy-start(f32[2048]{0:T(1024)} %param.14) | copy-start | bytes 24580
  6.5 53.7 %all-gather.4.cloned.1.call-start = ((), (), s32[]{:S(2)}) async-start(), calls=%async_computation.2 | async-start | bytes 2359296 | tf_op jit(solution)/shard_map/all_gather | solution.py:35
  19.1 3.5 %copy-start.2 = (bf16[1024,2048]{1,0:T(8,128)(2,1)S(1)}, bf16[1024,2048]{1,0:T(8,128)(2,1)}, u32[]{:S(2)}) copy-start(bf16[1024,2048]{1,0:T(8,128)(2,1)} %param.13) | copy-start | bytes 12582916
  22.5 1.0 %copy-start.4 = (bf16[2048,64]{0,1:T(8,128)(2,1)S(1)}, bf16[2048,64]{0,1:T(8,128)(2,1)}, u32[]{:S(2)}) copy-start(bf16[2048,64]{0,1:T(8,128)(2,1)} %param.17) | copy-start | bytes 786436
  23.6 10.1 %copy-start.1 = (bf16[1024,2048]{1,0:T(8,128)(2,1)}, bf16[1024,2048]{1,0:T(8,128)(2,1)S(1)}, u32[]{:S(2)}) copy-start(bf16[1024,2048]{1,0:T(8,128)(2,1)S(1)} %fusion.2) | copy-start | bytes 12582916
  23.6 1.4 %copy-start.5 = (bf16[2048,64]{0,1:T(8,128)(2,1)S(1)}, bf16[2048,64]{0,1:T(8,128)(2,1)}, u32[]{:S(2)}) copy-start(bf16[2048,64]{0,1:T(8,128)(2,1)} %param.16) | copy-start | bytes 786436
  25.0 7.4 %copy-start.10 = (bf16[2048,128]{1,0:T(8,128)(2,1)S(1)}, bf16[2048,128]{1,0:T(8,128)(2,1)}, u32[]{:S(2)}) copy-start(bf16[2048,128]{1,0:T(8,128)(2,1)} %param.20) | copy-start | bytes 1572868
  26.4 7.2 %copy-start.3 = (bf16[2048,128]{1,0:T(8,128)(2,1)S(1)}, bf16[2048,128]{1,0:T(8,128)(2,1)}, u32[]{:S(2)}) copy-start(bf16[2048,128]{1,0:T(8,128)(2,1)} %param.19) | copy-start | bytes 1572868
  26.4 33.8 %collective-permute-start = (bf16[128,128]{0,1:T(8,128)(2,1)S(1)}, bf16[128,128]{0,1:T(8,128)(2,1)S(1)}, u32[]{:S(2)}, u32[]{:S(2)}) collective-permute-start(bf16[128,128]{0,1:T(8,128)(2,1)S(1)} %fusion.53), channel_id=1, source_target_pairs={{0,4},{4,8},{8,12},{12,16},{16,20},{20,24},{24,28},{28,32},{32,36}... | collective-permute-start | bytes 98312 | tf_op jit(solution)/shard_map/ppermute | solution.py:23
  33.7 4.3 %copy-start.11 = (bf16[2048,128]{1,0:T(8,128)(2,1)S(1)}, bf16[2048,128]{1,0:T(8,128)(2,1)}, u32[]{:S(2)}) copy-start(bf16[2048,128]{1,0:T(8,128)(2,1)} %param.15) | copy-start | bytes 1572868
  34.9 6.5 %copy-start.7 = (f32[1024]{0:T(1024)S(1)}, f32[1024]{0:T(1024)}, u32[]{:S(2)}) copy-start(f32[1024]{0:T(1024)} %param.24) | copy-start | bytes 12292
  35.0 6.8 %collective-permute-start.1 = (bf16[30,128]{1,0:T(8,128)(2,1)S(1)}, bf16[30,128]{1,0:T(8,128)(2,1)S(1)}, u32[]{:S(2)}, u32[]{:S(2)}) collective-permute-start(bf16[30,128]{1,0:T(8,128)(2,1)S(1)} %slice.290), channel_id=1, source_target_pairs={{0,4},{4,8},{8,12},{12,16},{16,20},{20,24},{24,28},{28,32},{32,36}... | collective-permute-start | bytes 23048 | tf_op jit(solution)/shard_map/ppermute | solution.py:23
  44.8 18.5 %all-to-all-start.1 = ((bf16[4,256,128]{1,2,0:T(8,128)(2,1)}), bf16[4,256,128]{1,2,0:T(8,128)(2,1)S(1)}, u32[]{:S(2)}, u32[]{:S(2)}) async-start(bf16[4,256,128]{1,2,0:T(8,128)(2,1)} %copy.43), calls=%async_computation.1 | async-start | bytes 524288 | tf_op jit(solution)/shard_map/all_to_all | solution.py:154
  48.5 12.7 %copy-start.9 = (f32[2]{0:T(128)S(1)}, f32[2]{0:T(128)}, u32[]{:S(2)}) copy-start(f32[2]{0:T(128)} %param.18) | copy-start | bytes 28
  48.5 36.0 %all-gather.6.cloned.1.call-start = ((), (), s32[]{:S(2)}) async-start(), calls=%async_computation.3 | async-start | bytes 6291456 | tf_op jit(solution)/shard_map/all_gather | solution.py:35
  61.7 5.8 %copy-start.8 = (f32[512]{0:T(512)S(1)}, f32[512]{0:T(512)}, u32[]{:S(2)}) copy-start(f32[512]{0:T(512)} %param.22) | copy-start | bytes 6148
  63.3 9.5 %all-to-all-start = ((bf16[4,256,128]{1,2,0:T(8,128)(2,1)}), bf16[4,256,128]{1,2,0:T(8,128)(2,1)S(1)}, u32[]{:S(2)}, u32[]{:S(2)}) async-start(bf16[4,256,128]{1,2,0:T(8,128)(2,1)} %copy.41), calls=%async_computation | async-start | bytes 524288 | tf_op jit(solution)/shard_map/all_to_all | solution.py:153
Sparse Core Ops, SparseCore 0:
  19.2 40.9 all-gather.3
  62.0 22.4 all-gather.5
where the time goes:
time: 96.6 us; the launch traced here: 96.1 us
  waiting for transfers between devices  27.6 us (29%)
  starting transfers between devices  15.6 us (16%)
  between operations  13.8 us (14%)
  blocking collectives  12.5 us (13%)
  matrix products  12.4 us (13%)
  other arithmetic  8.87 us (9%)
  local copies, waits for them, and re-layouts  5.36 us (6%)
    all_gather x2, waiting for transfers between devices, stacked_from(): tiles = lax.all_gather(tiles, axes[k], axis=0, tiled=True)  23 us
    all_gather x1, blocking collectives, stacked_from(): tiles = lax.all_gather(tiles, axes[k], axis=0, tiled=True)  12.5 us
    ppermute x2, starting transfers between devices, from_behind(): return lax.ppermute(block, axis, route)  7.83 us
    all_to_all x1, waiting for transfers between devices, on_device(): lax.all_to_all(attended, 'tp', split_axis=0, concat_axis=1, tiled=True)  4.52 us
    all_to_all x1, starting transfers between devices, on_device(): lax.all_to_all(attended, 'tp', split_axis=0, concat_axis=1, tiled=True)  3.98 us
    all_to_all x1, starting transfers between devices, on_device(): lax.all_to_all(second, 'tp', split_axis=0, concat_axis=1, tiled=True)  3.75 us
    dot_general x1, matrix products, on_device(): jnp.dot(normed, query_weight, preferred_element_type=jnp.float32)  3.45 us
    reduce_sum x2, other arithmetic, rms_rows(): jnp.mean(values * values, axis=-1, keepdims=True) + NORM_EPSILON  3.32 us
  transfers between devices with their start and end apart: 6, of which 3 were waited for; matrix products, arithmetic and copies ran while one was open for 22% of the time, Pallas kernels for 0%

commit v1 on v0

v1 whole, which is shorter than its diff:
```python
import jax
import jax.numpy as jnp
from jax import lax
from jax.experimental import pallas as pl
from jax.experimental.pallas import tpu as pltpu
from jax.sharding import Mesh
from jax.sharding import PartitionSpec as P

NZ, NX, NC, NY = 8, 4, 2, 4
D = 2048
HEAD_DIM = 64
WINDOW = 128
TAPS = 31
ROWS = 1024
QROWS = 256
LANES = 128
MIX_HALF = 512
SHARD = 16
PART_A = 1280
PART_B = D - PART_A
EPS = 1e-06
NEG = -1e30
F32 = jnp.float32
BF16 = jnp.bfloat16
CHUNKS = (3, 0, 1, 2)
N_REMOTE = 72
N_LOCAL = 24


def kernel(
    tok, gain, wq, wk, wv, sink, wci, wcg, taps, cgain, pw, ogain, ow, out,
    xb, nb, wcat, wkb, wvb, gainb, sinkb, tapb, cgainb, pwb, ogainb, wa, wb,
    qs, kvs, gs, att_s, cv_s, att_r, cv_r, act, merged, ob,
    send_sem, recv_sem, loc_sem,
):
    z = lax.axis_index("z")
    x = lax.axis_index("x")
    c = lax.axis_index("c")
    y = lax.axis_index("y")
    sp = (z * NX + x) * NC + c

    def zr(d):
        return lax.rem(z + (d % NZ), NZ)

    def xr(d):
        return lax.rem(x + (d % NX), NX)

    def yr(d):
        return lax.rem(y + (d % NY), NY)

    def dev(dz=0, dx=0, dy=0):
        return {"z": zr(dz), "x": xr(dx), "c": c, "y": yr(dy)}

    def at_sp(s):
        return {"z": s // (NX * NC), "x": (s // NC) % NX, "c": s % NC, "y": y}

    sibling = {"z": z, "x": x, "c": 1 - c, "y": y}
    after = at_sp(lax.rem(sp + 1, NZ * NX * NC))
    before = at_sp(lax.rem(sp + NZ * NX * NC - 1, NZ * NX * NC))

    local_count = [0]

    def local(src, dst):
        copy = pltpu.make_async_copy(src, dst, loc_sem.at[local_count[0]])
        local_count[0] += 1
        copy.start()
        return copy

    remote_count = [0]
    sent = []

    def remote(src, dst, to):
        i = remote_count[0]
        remote_count[0] += 1
        copy = pltpu.make_async_remote_copy(
            src_ref=src, dst_ref=dst, send_sem=send_sem.at[i], recv_sem=recv_sem.at[i],
            device_id=to, device_id_type=pl.DeviceIdType.MESH,
        )
        copy.start()
        sent.append(copy)
        return copy

    own_a = local(ow.at[:, 0:PART_A], wa.at[z, x, c])
    own_b = local(ow.at[:, PART_A:D], wb.at[z, x, c])

    def rows_of(chunk):
        return pl.ds(chunk * QROWS, QROWS)

    tok_copies = {}
    first = CHUNKS[0]
    tok_copies[first] = local(tok.at[rows_of(first)], xb.at[rows_of(first)])
    gain_copy = local(gain, gainb)
    w_copies = [
        local(wk, wkb),
        local(wv, wvb),
        local(wq, wcat.at[:, 0:128]),
        local(wci, wcat.at[:, 128:256]),
        local(wcg, wcat.at[:, 256:384]),
    ]
    for chunk in CHUNKS[1:]:
        tok_copies[chunk] = local(tok.at[rows_of(chunk)], xb.at[rows_of(chunk)])
    late = [
        local(sink, sinkb),
        local(taps.at[:, pl.ds(pl.multiple_of(y * LANES, LANES), LANES)], tapb),
        local(cgain, cgainb),
        local(ogain, ogainb),
        local(pw, pwb),
    ]

    barrier = pltpu.get_barrier_semaphore()
    partners = [dev(dz=d) for d in (1, -1, 2, -2)]
    partners += [dev(dx=d) for d in (1, -1, 2)]
    partners += [dev(dy=d) for d in (1, -1, 2)]
    partners += [sibling, after, before]
    for partner in partners:
        pl.semaphore_signal(barrier, inc=1, device_id=partner, device_id_type=pl.DeviceIdType.MESH)
    pl.semaphore_wait(barrier, len(partners))

    def move_a(rz, rx, dz, dx):
        block = wa.at[zr(rz), xr(rx), c]
        return remote(block, block, dev(dz=dz, dx=dx))

    def move_b(rx, dx):
        block = wb.at[z, xr(rx), c]
        return remote(block, block, dev(dx=dx))

    def move_row(rz, dz):
        block = wb.at[zr(rz), :, c]
        return remote(block, block, dev(dz=dz))

    def share_a(rz):
        block = wa.at[zr(rz), :, c]
        return remote(block, block, sibling)

    def share_b(rz):
        block = wb.at[zr(rz), :, c]
        return remote(block, block, sibling)

    gather = {}

    def stage0():
        own_a.wait()
        gather["t1"] = [move_a(0, 0, d, 0) for d in (1, -1, 2, -2)]
        own_b.wait()
        gather["bx"] = [move_b(0, d) for d in (1, -1, 2)]
        gather["ax0"] = [move_a(0, 0, 0, d) for d in (1, -1, 2)]

    def stage1():
        for copy in gather["bx"] + gather["t1"]:
            copy.wait_recv()
        gather["t2"] = [move_a(-2, 0, 1, 0), move_a(2, 0, -1, 0), move_a(-2, 0, 2, 0)]
        gather["r1"] = [move_row(0, d) for d in (1, -1, 2, -2)]
        gather["ax1"] = [move_a(rz, 0, 0, d) for rz in (1, -1, 2, -2) for d in (1, -1, 2)]
        gather["sb0"] = [share_b(0)]

    def stage2():
        for copy in gather["t2"] + gather["r1"] + gather["ax0"]:
            copy.wait_recv()
        gather["r2"] = [move_row(-2, 1), move_row(2, -1), move_row(-2, 2)]
        gather["ax2"] = [move_a(rz, 0, 0, d) for rz in (3, -3, -4) for d in (1, -1, 2)]
        gather["sb1"] = [share_b(rz) for rz in (1, -1, 2, -2)]
        gather["sa0"] = [share_a(0)]

    def stage3():
        for copy in gather["ax1"]:
            copy.wait_recv()
        gather["sa1"] = [share_a(rz) for rz in (1, -1, 2, -2)]

    def stage4():
        for copy in gather["r2"] + gather["ax2"]:
            copy.wait_recv()
        gather["sb2"] = [share_b(rz) for rz in (3, -3, -4)]
        gather["sa2"] = [share_a(rz) for rz in (3, -3, -4)]

    stage0()

    def norm(chunk, slot):
        for sub in range(QROWS // 16):
            wide = xb[pl.ds(chunk * QROWS + sub * 16, 16), :].astype(F32)
            mean = jnp.mean(wide * wide, axis=-1, keepdims=True)
            value = wide * lax.rsqrt(mean + EPS) * gainb[...]
            nb[slot, pl.ds(sub * 16, 16), :] = value.astype(BF16)

    lane = lax.broadcasted_iota(jnp.int32, (QROWS, LANES), 1)
    halves = {}

    def project(chunk, slot):
        return jnp.dot(nb[slot], wcat[...], preferred_element_type=F32)

    def keep(chunk, result):
        query = result[:, 0:128]
        low = jnp.where(lane < HEAD_DIM, query, 0.0).astype(BF16)
        high = jnp.where(lane < HEAD_DIM, pltpu.roll(query, HEAD_DIM, 1), 0.0).astype(BF16)
        for j in range(2):
            block = chunk * 2 + j
            qs[pl.ds(block * 256, 128), :] = low[j * 128 : (j + 1) * 128]
            qs[pl.ds(block * 256 + 128, 128), :] = high[j * 128 : (j + 1) * 128]
        gated = result[:, 128:256] * jax.nn.sigmoid(result[:, 256:384])
        gs[pl.ds(32 + chunk * QROWS, QROWS), :] = gated.astype(BF16).astype(F32)
        kvs[pl.ds(WINDOW + chunk * QROWS, QROWS), :] = result[:, 384:512].astype(BF16)

    gain_copy.wait()
    tok_copies[first].wait()
    norm(first, 0)
    for copy in w_copies:
        copy.wait()
    wcat[:, 384:512] = jnp.concatenate([wkb[...], wvb[...]], axis=1)
    halo = []
    for i, chunk in enumerate(CHUNKS):
        if i + 1 < len(CHUNKS):
            tok_copies[CHUNKS[i + 1]].wait()
        result = project(chunk, i % 2)
        if i + 1 < len(CHUNKS):
            norm(CHUNKS[i + 1], (i + 1) % 2)
        keep(chunk, result)
        if i == 0:
            halo.append(remote(kvs.at[pl.ds(ROWS, WINDOW)], kvs.at[pl.ds(0, WINDOW)], after))
            halo.append(remote(gs.at[pl.ds(ROWS, 32)], gs.at[pl.ds(0, 32)], after))
        if i == 1:
            stage1()
    for copy in late:
        copy.wait()
    for copy in halo:
        copy.wait_recv()

    @pl.when(sp == 0)
    def _():
        kvs[pl.ds(0, WINDOW), :] = jnp.zeros((WINDOW, LANES), BF16)
        gs[pl.ds(0, 32), :] = jnp.zeros((32, LANES), F32)

    row = lax.broadcasted_iota(jnp.int32, (WINDOW, WINDOW), 0)
    col = lax.broadcasted_iota(jnp.int32, (WINDOW, WINDOW), 1)
    ahead = col - row
    earlier = ahead > 0

    def attend(block, store):
        keys = kvs[pl.ds(pl.multiple_of(block * WINDOW, WINDOW), 2 * WINDOW), :]
        query = qs[pl.ds(pl.multiple_of(block * 256, 256), 256), :]
        scores = lax.dot_general(
            query, keys, (((1,), (1,)), ((), ())), preferred_element_type=F32
        )
        opening = jnp.where(jnp.logical_and(sp == 0, block == 0), 1, 0)
        closed = ahead * opening > 0
        shares = []
        for h in range(2):
            rows = slice(h * 128, (h + 1) * 128)
            both = jnp.where(earlier, scores[rows, 0:128], scores[rows, 128:256]) * HEAD_DIM ** (-0.5)
            both = jnp.where(closed, NEG, both)
            logit = sinkb[h]
            top = jnp.maximum(jnp.max(both, axis=-1, keepdims=True), logit)
            raised = jnp.exp(both - top)
            total = jnp.sum(raised, axis=-1, keepdims=True) + jnp.exp(logit - top)
            weight = raised * (1.0 / total)
            shares.append(
                jnp.concatenate(
                    [jnp.where(earlier, weight, 0.0), jnp.where(earlier, 0.0, weight)], axis=1
                ).astype(BF16)
            )
        mixed = jnp.dot(jnp.concatenate(shares, axis=0), keys, preferred_element_type=F32)
        lane_here = lax.broadcasted_iota(jnp.int32, (WINDOW, LANES), 1)
        joined = jnp.where(lane_here < HEAD_DIM, pltpu.roll(mixed[0:128], HEAD_DIM, 1), mixed[128:256])
        store(joined.astype(BF16))

    def convolve(quarter, store):
        base = quarter * QROWS
        for sub in range(QROWS // 64):
            total = jnp.zeros((64, LANES), F32)
            for k in range(TAPS):
                total = total + tapb[k : k + 1, :].astype(F32) * gs[pl.ds(base + sub * 64 + 2 + k, 64), :]
            store(sub, total.astype(BF16))

    exchange_att = []
    exchange_cv = []
    for step, turn in enumerate((2, 1, -1, 0)):
        quarter = yr(turn)
        for j in range(2):
            def keep_att(value, j=j):
                if turn == 0:
                    att_r[y, j * 128 : (j + 1) * 128, :] = value
                else:
                    att_s[step, j * 128 : (j + 1) * 128, :] = value

            attend(quarter * 2 + j, keep_att)
        if turn != 0:
            exchange_att.append(remote(att_s.at[step], att_r.at[y], dev(dy=turn)))

        def keep_cv(sub, value):
            if turn == 0:
                cv_r[y, sub * 64 : (sub + 1) * 64, :] = value
            else:
                cv_s[step, sub * 64 : (sub + 1) * 64, :] = value

        convolve(quarter, keep_cv)
        if turn != 0:
            exchange_cv.append(remote(cv_s.at[step], cv_r.at[y], dev(dy=turn)))
        if step == 0:
            stage2()
        if step == 2:
            stage3()

    for copy in exchange_att:
        copy.wait_recv()
    for sub in range(QROWS // 32):
        rows = pl.ds(sub * 32, 32)
        pieces = [att_r[j, rows, :].astype(F32) for j in range(NY)]
        square = sum(jnp.sum(p * p, axis=-1, keepdims=True) for p in pieces)
        scale = lax.rsqrt(square * (1.0 / MIX_HALF) + EPS)
        for j in range(NY):
            cols = slice(j * 128, (j + 1) * 128)
            merged[rows, cols] = (pieces[j] * scale * ogainb[:, cols]).astype(BF16)
    for copy in exchange_cv:
        copy.wait_recv()
    for sub in range(QROWS // 32):
        rows = pl.ds(sub * 32, 32)
        pieces = [cv_r[j, rows, :].astype(F32) for j in range(NY)]
        mean = sum(jnp.sum(p, axis=-1, keepdims=True) for p in pieces) * (1.0 / MIX_HALF)
        pieces = [p - mean for p in pieces]
        square = sum(jnp.sum(p * p, axis=-1, keepdims=True) for p in pieces)
        scale = lax.rsqrt(square * (1.0 / MIX_HALF) + EPS)
        for j in range(NY):
            cols = slice(j * 128, (j + 1) * 128)
            scaled = pieces[j] * scale * cgainb[:, cols]
            act[rows, cols] = (scaled * jax.nn.sigmoid(scaled)).astype(BF16)
    point = jnp.dot(act[...], pwb[...], preferred_element_type=F32)
    square = jnp.sum(point * point, axis=-1, keepdims=True)
    scale = lax.rsqrt(square * (1.0 / MIX_HALF) + EPS)
    merged[:, MIX_HALF:] = (point * scale * ogainb[:, MIX_HALF:]).astype(BF16)

    stage4()
    for name in ("sb0", "sb1", "sb2", "sa0", "sa1", "sa2"):
        for copy in gather[name]:
            copy.wait_recv()
    outs = []
    for start in range(0, D, 256):
        if start < PART_A:
            block = wa[:, :, :, :, start : start + 256]
        else:
            block = wb[:, :, :, :, start - PART_A : start - PART_A + 256]
        ob[:, start : start + 256] = jnp.dot(
            merged[...], block.reshape(2 * MIX_HALF, 256), preferred_element_type=F32
        ).astype(BF16)
        if start % 512 == 256:
            cols = pl.ds(start - 256, 512)
            outs.append(local(ob.at[:, cols], out.at[:, cols]))
    for copy in outs:
        copy.wait()
    for copy in sent:
        copy.wait_send()


def on_device(
    tokens, norm_gain, query_weight, key_weight, value_weight, sink_logits, conv_in_weight,
    conv_gate_weight, conv_taps, conv_gain, point_weight, output_gain, output_weight,
):
    anywhere = pl.BlockSpec(memory_space=pl.ANY)
    return pl.pallas_call(
        kernel,
        name="mixer",
        out_shape=jax.ShapeDtypeStruct((QROWS, D), BF16),
        in_specs=[anywhere] * 13,
        out_specs=anywhere,
        scratch_shapes=[
            pltpu.VMEM((ROWS, D), BF16),
            pltpu.VMEM((2, QROWS, D), BF16),
            pltpu.VMEM((D, 512), BF16),
            pltpu.VMEM((D, 64), BF16),
            pltpu.VMEM((D, 64), BF16),
            pltpu.VMEM((1, D), F32),
            pltpu.SMEM((2,), F32),
            pltpu.VMEM((TAPS, LANES), BF16),
            pltpu.VMEM((1, MIX_HALF), F32),
            pltpu.VMEM((MIX_HALF, MIX_HALF), BF16),
            pltpu.VMEM((1, 2 * MIX_HALF), F32),
            pltpu.VMEM((NZ, NX, NC, SHARD, PART_A), BF16),
            pltpu.VMEM((NZ, NX, NC, SHARD, PART_B), BF16),
            pltpu.VMEM((2 * ROWS, LANES), BF16),
            pltpu.VMEM((WINDOW + ROWS, LANES), BF16),
            pltpu.VMEM((32 + ROWS, LANES), F32),
            pltpu.VMEM((NY - 1, QROWS, LANES), BF16),
            pltpu.VMEM((NY - 1, QROWS, LANES), BF16),
            pltpu.VMEM((NY, QROWS, LANES), BF16),
            pltpu.VMEM((NY, QROWS, LANES), BF16),
            pltpu.VMEM((QROWS, MIX_HALF), BF16),
            pltpu.VMEM((QROWS, 2 * MIX_HALF), BF16),
            pltpu.VMEM((QROWS, D), BF16),
            pltpu.SemaphoreType.DMA((N_REMOTE,)),
            pltpu.SemaphoreType.DMA((N_REMOTE,)),
            pltpu.SemaphoreType.DMA((N_LOCAL,)),
        ],
        compiler_params=pltpu.CompilerParams(
            collective_id=0, has_side_effects=True, vmem_limit_bytes=60 * 1024 * 1024
        ),
    )(
        tokens, norm_gain.reshape(1, D), query_weight, key_weight, value_weight, sink_logits,
        conv_in_weight, conv_gate_weight, conv_taps, conv_gain.reshape(1, MIX_HALF), point_weight,
        output_gain.reshape(1, 2 * MIX_HALF), output_weight,
    )


def solution(mesh):
    split = Mesh(mesh.devices.reshape(NZ, NX, NC, NY), ("z", "x", "c", "y"))
    sp = ("z", "x", "c")
    in_specs = (
        P(sp, None), P(), P(None, "y"), P(None, "y"), P(None, "y"), P("y"), P(None, "y"),
        P(None, "y"), P(), P(), P(), P(), P(sp, None),
    )
    return jax.shard_map(
        on_device, mesh=split, in_specs=in_specs, out_specs=P(("z", "x", "c", "y"), None),
        check_vma=False,
    )
```

time: 96.6 us -> 44.5 us (0.46)
  Pallas kernels: 0 us -> 38 us
  waiting for transfers between devices: 27.6 us -> 0 us
  starting transfers between devices: 15.6 us -> 0 us
  between operations: 13.8 us -> 0.01 us
  blocking collectives: 12.5 us -> 0 us
  matrix products: 12.4 us -> 0 us
  other arithmetic: 8.87 us -> 0 us
    pallas_call x0 -> x1, Pallas kernels: none -> 38 us  [on_device(): pl.pallas_call(kernel, name='mixer', out_shape=jax.ShapeDtypeStruct((QROW...]
    all_gather x2 -> x0, waiting for transfers between devices: 23 us -> none  [stacked_from(): tiles = lax.all_gather(tiles, axes[k], axis=0, tiled=True)]
    all_gather x1 -> x0, blocking collectives: 12.5 us -> none  [stacked_from(): tiles = lax.all_gather(tiles, axes[k], axis=0, tiled=True)]
    dot_general x9 -> x0, matrix products: 12.4 us -> none  [the longest x1 3.45 us: on_device(): jnp.dot(normed, query_weight, preferred_element_type=jnp.float32)]
    ppermute x2 -> x0, starting transfers between devices: 7.83 us -> none  [from_behind(): return lax.ppermute(block, axis, route)]
    all_to_all x2 -> x0, starting transfers between devices: 7.73 us -> none  [the longest x1 3.98 us: on_device(): lax.all_to_all(attended, 'tp', split_axis=0, concat_axis=1, tiled=True)]
    unnamed x27 -> x3, local copies, waits for them, and re-layouts: 0.39 us -> 6.23 us
    all_to_all x2 -> x0, waiting for transfers between devices: 4.52 us -> none  [the longest x1 4.52 us: on_device(): lax.all_to_all(attended, 'tp', split_axis=0, concat_axis=1, tiled=True)]
  transfers between devices with their start and end apart: 6 -> 0, of which waited for: 3 -> 0; matrix products, arithmetic and copies ran while one was open for 22% -> 0% of each run, Pallas kernels for 0% -> 0%
where the time goes in v1:
time: 44.5 us; the launch traced here: 44.3 us
  Pallas kernels  38 us (85%)
  local copies, waits for them, and re-layouts  6.23 us (14%)
    pallas_call x1, Pallas kernels, on_device(): pl.pallas_call(kernel, name='mixer', out_shape=jax.ShapeDtypeStruct((QROW...  38 us
    unnamed x3, local copies, waits for them, and re-layouts  6.23 us

profile of v1, /device:TPU:1, one launch (start us, length us, event | category | flops | bytes accessed | tf_op | source)
XLA Modules:
  0.0 44.3 jit_solution(269106561348755816)
XLA Ops:
  0.0 2.0 %copy.14.wk = bf16[2048,64]{1,0:T(8,128)(2,1)} copy(bf16[2048,64]{0,1:T(8,128)(2,1)} %param.16) | data formatting | bytes 524288 | tf_op args[3]
  2.0 2.0 %copy.15.wv = bf16[2048,64]{1,0:T(8,128)(2,1)} copy(bf16[2048,64]{0,1:T(8,128)(2,1)} %param.17) | data formatting | bytes 524288 | tf_op args[4]
  3.9 38.0 %mixer.1 = bf16[256,2048]{1,0:T(8,128)(2,1)} custom-call(bf16[1024,2048]{1,0:T(8,128)(2,1)} %tok.1, f32[1,2048]{1,0:T(1,128)} %bitcast.3, bf16[2048,128]{1,0:T(8,128)(2,1)} %wq.1, bf16[2048,64]{1,0:T(8,128)(2,1)} %copy.14.wk, bf16[2048,64]{1,0:T(8,128)(2,1)} %copy.15.wv, f32[2]{0:T(128)} %sink.1, bf16[2048,128]{1,0:T(8,128)(2,1)} %wci.1, ...), custom_call_target="tpu_custom_call" | custom-call | tf_op jit(solution)/shard_map/mixer/pallas_call | solution.py:356
  42.0 2.3 %copy.17 = bf16[256,2048]{1,0:T(8,128)(2,1)} copy(bf16[256,2048]{1,0:T(8,128)(2,1)} %mixer.1) | data formatting | bytes 2097152
